TPU v7x, 256 devices: a 8x8x2 block of a 8x8x16 slice. The times are simulated.
256 devices in a mesh: grp: 2 (over z), ep: 64 (over y, x), tp: 2 (over core).
Axes of the slice: x: 8, y: 8, z: 2, core: 2. Of those that a mesh axis runs over, the one named last changes fastest.
The devices are a block of a 8x8x16 slice.
Arguments:
- tokens: bfloat16 [16384, 2048], P(('grp', 'ep', 'tp')), parts along dimension 0, may hold values from -6 to 6
- norm_gain: float32 [2048], replicated, may hold values from 0.1 to 1.9
- expert_ids: int32 [16384, 2], P(('grp', 'ep', 'tp')), parts along dimension 0, may hold values from 0 to 15, all different within a row; in each aligned block of 64 rows (0 to 63, 64 to 127, ...) at most 10 rows name the same one
- gate_weights: float32 [16384, 2], P(('grp', 'ep', 'tp')), parts along dimension 0, may hold values from 0.2 to 1
- w_gate: bfloat16 [2048, 114688], P(None, ('ep', 'tp')), may hold values from -0.125 to 0.125
- w_up: bfloat16 [2048, 114688], P(None, ('ep', 'tp')), may hold values from -0.125 to 0.125
- w_down: bfloat16 [114688, 2048], P(('ep', 'tp')), may hold values from -0.0625 to 0.0625
Outputs:
- mixed: bfloat16 [16384, 2048], P(('grp', 'ep', 'tp')), parts along dimension 0
There are 2 independent parts, one for each index of `grp`. A program takes and returns all parts, laid end to end along the dimension named above; an argument that names none is the same for every part. Nothing has to cross between parts.
Inputs may be any that keep to these rules, and one draw needn't show every extreme that they name: `expert_ids`: each token names 2 different experts. Among the rows of one device no expert is named by more than 10 rows, a bound that some blocks reach; every expert is named somewhere.
All inputs are finite; a program needn't handle non-finite values.
Results may differ from a plain program's by a relative error of at most 0.0095.
Values may be sent and summed in bfloat16 or wider, within the bound.
No kernel may reach another device: no remote copies, remote signals or barrier semaphores. Data moves between devices by JAX's collectives and lax.ppermute only.
A program may use at most 192 MiB of HBM per device.

v0:
```python
import jax
import jax.numpy as jnp
from jax import lax
from jax.sharding import PartitionSpec as P

GROUP = 4


def layer_norm(tokens, norm_gain):
    values = tokens.astype(jnp.float32)
    center = jnp.mean(values, -1, keepdims=True)
    spread = jnp.mean(jnp.square(values - center), -1, keepdims=True)
    return ((values - center) * lax.rsqrt(spread + 1e-05) * norm_gain).astype(jnp.bfloat16)


def rounded(values):
    return lax.optimization_barrier(values.astype(jnp.bfloat16)).astype(jnp.float32)


def per_device(tokens, norm_gain, expert_ids, gate_weights, w_gate, w_up, w_down):
    ep_devices = lax.axis_size("ep")
    local_rows, width = tokens.shape
    picks = expert_ids.shape[1]
    experts = ep_devices // GROUP
    capacity = max(2, min(local_rows, local_rows * picks * 4 // (3 * experts)))
    normed = layer_norm(tokens, norm_gain)
    flat_ids = expert_ids.reshape(-1)
    matches = (flat_ids[:, None] == jnp.arange(experts, dtype=jnp.int32)[None, :]).astype(jnp.int32)
    position = jnp.sum((jnp.cumsum(matches, 0) - 1) * matches, 1)
    target = flat_ids * capacity + position
    source = jnp.arange(local_rows * picks, dtype=jnp.int32) // picks
    packed = jnp.zeros((experts * capacity, width), jnp.bfloat16).at[target].set(normed[source])
    copies = jnp.broadcast_to(
        packed.reshape(experts, 1, capacity, width), (experts, GROUP, capacity, width)
    )
    copies = copies.reshape(ep_devices, capacity, width)
    arrived = lax.all_to_all(copies, "ep", split_axis=0, concat_axis=0, tiled=True).reshape(
        ep_devices * capacity, width
    )
    gate_all, up_all = (
        lax.all_gather(w_gate, "tp", axis=1, tiled=True),
        lax.all_gather(w_up, "tp", axis=1, tiled=True),
    )
    down_all = lax.all_gather(w_down, "tp", axis=0, tiled=True)
    gate_part = jnp.dot(arrived, gate_all, preferred_element_type=jnp.float32)
    up_part = jnp.dot(arrived, up_all, preferred_element_type=jnp.float32)
    hidden = (jax.nn.silu(gate_part) * up_part).astype(jnp.bfloat16)
    block_width = w_gate.shape[1]
    summed = jnp.zeros((ep_devices * capacity, width), jnp.float32)
    for side_index in range(lax.axis_size("tp")):
        lower = side_index * block_width
        summed = summed + rounded(
            jnp.dot(
                hidden[:, lower : lower + block_width],
                down_all[lower : lower + block_width],
                preferred_element_type=jnp.float32,
            )
        )
    partial_value = summed.astype(jnp.bfloat16).reshape(ep_devices, capacity, width)
    returned = lax.all_to_all(partial_value, "ep", split_axis=0, concat_axis=0, tiled=True)
    grouped = jnp.sum(returned.reshape(experts, GROUP, capacity, width).astype(jnp.float32), 1)
    grouped = grouped.reshape(experts * capacity, width)
    picked = grouped[target] * gate_weights.reshape(-1)[:, None]
    return jnp.sum(picked.reshape(local_rows, picks, width), 1).astype(jnp.bfloat16)


def solution(mesh):
    in_specs = (
        P(("grp", "ep", "tp"), None),
        P(),
        P(("grp", "ep", "tp"), None),
        P(("grp", "ep", "tp"), None),
        P(None, ("ep", "tp")),
        P(None, ("ep", "tp")),
        P(("ep", "tp"), None),
    )
    out_specs = P(("grp", "ep", "tp"), None)
    return jax.shard_map(
        per_device, mesh=mesh, in_specs=in_specs, out_specs=out_specs, check_vma=False
    )
```

profile of v0, /device:TPU:668, one launch (start us, length us, event | category | flops | bytes accessed | tf_op | source)
XLA Modules:
  0.0 360.3 jit_solution(2860947420082868165)
XLA Ops:
  6.6 0.7 all-gather.4.cloned.1.call-update
  7.4 0.7 all-gather.6.cloned.1.call-update
  9.2 0.2 fusion.14
  9.7 3.2 scatter_custom_fusion
  12.9 0.2 broadcast_in_dim.7
  13.1 2.6 broadcast_in_dim.8
  15.7 18.2 %all-to-all-start = ((bf16[64,10,2048]{2,1,0:T(8,128)(2,1)}), bf16[64,10,2048]{2,1,0:T(8,128)(2,1)}, u32[]{:S(2)}, u32[]{:S(2)}) async-start(bf16[64,10,2048]{2,1,0:T(8,128)(2,1)} %bitcast.16), calls=%async_computation | async-start | bytes 8388608 | tf_op jit(solution)/shard_map/all_to_all | solution.py:37
  33.9 0.2 all-gather.8.cloned.1.call-start
  34.2 0.5 all-gather.8.cloned.1.call-update
  34.7 123.9 %all-to-all-done = bf16[64,10,2048]{2,1,0:T(8,128)(2,1)} async-done(((bf16[64,10,2048]{2,1,0:T(8,128)(2,1)}), bf16[64,10,2048]{2,1,0:T(8,128)(2,1)}, u32[]{:S(2)}, u32[]{:S(2)}) %all-to-all-start) | async-done | bytes 2621472 | tf_op jit(solution)/shard_map/all_to_all | solution.py:37
  158.7 4.1 %reshape.112 = bf16[640,2048]{1,0:T(8,128)(2,1)S(1)} reshape(bf16[64,10,2048]{2,1,0:T(8,128)(2,1)} %all-to-all-done) | data formatting | bytes 5242880 | tf_op jit(solution)/shard_map/reshape | solution.py:37
  162.8 9.7 %fusion.23 = f32[640,1792]{1,0:T(8,128)} fusion(bf16[640,2048]{1,0:T(8,128)(2,1)S(1)} %reshape.112, bf16[2048,1792]{1,0:T(8,128)(2,1)} %all-gather.4.cloned.1.call-done), kind=kOutput, calls=%fused_computation.42 | convolution fusion | flops 4697620480 | bytes 14548992 | tf_op jit(solution)/shard_map/dot_general | solution.py:45
  172.4 10.0 %multiply_convert_fusion = bf16[640,1792]{1,0:T(8,128)(2,1)} fusion(f32[640,1792]{1,0:T(8,128)} %fusion.23, bf16[640,2048]{1,0:T(8,128)(2,1)S(1)} %reshape.112, bf16[2048,1792]{1,0:T(8,128)(2,1)} %all-gather.6.cloned.1.call-done), kind=kOutput, calls=%fused_computation.5 | convolution fusion | flops 4704501760 | bytes 16842752 | tf_op jit(solution)/shard_map/dot_general | solution.py:46
  182.4 5.4 %fusion.4 = bf16[640,2048]{1,0:T(8,128)(2,1)S(1)} fusion(bf16[1792,2048]{1,0:T(8,128)(2,1)} %all-gather.8.cloned.1.call-done, bf16[640,1792]{1,0:T(8,128)(2,1)} %multiply_convert_fusion), kind=kOutput, calls=%fused_computation.10 | convolution fusion | flops 2350120960 | bytes 7438336 | tf_op jit(solution)/shard_map/dot_general | solution.py:53
  187.9 3.1 fusion.7
  191.0 1.2 add_convert_fusion
  192.2 2.8 reshape.113
  194.9 9.5 %all-to-all-start.1 = ((bf16[64,10,2048]{2,1,0:T(8,128)(2,1)}), bf16[64,10,2048]{2,1,0:T(8,128)(2,1)}, u32[]{:S(2)}, u32[]{:S(2)}) async-start(bf16[64,10,2048]{2,1,0:T(8,128)(2,1)} %reshape.113), calls=%async_computation.1 | async-start | bytes 8388608 | tf_op jit(solution)/shard_map/all_to_all | solution.py:60
  204.6 141.8 %all-to-all-done.1 = bf16[64,10,2048]{2,1,0:T(8,128)(2,1)} async-done(((bf16[64,10,2048]{2,1,0:T(8,128)(2,1)}), bf16[64,10,2048]{2,1,0:T(8,128)(2,1)}, u32[]{:S(2)}, u32[]{:S(2)}) %all-to-all-start.1) | async-done | bytes 2621472 | tf_op jit(solution)/shard_map/all_to_all | solution.py:60
  346.4 3.3 convert_reduce_fusion
  349.6 0.2 reshape.114
  349.8 1.0 gather_fusion
  350.8 0.6 gather.10
  351.5 2.3 multiply_reduce_fusion
  (34 shorter events, 1.5 us)
Async XLA Ops:
  6.5 1.6 copy-start.2
  6.5 2.5 copy-start
  6.6 2.9 copy-start.1
  6.6 156.2 %all-gather.4.cloned.1.call-start = ((), (), s32[]{:S(2)}) async-start(), calls=%async_computation.2 | async-start | bytes 11010048 | tf_op jit(solution)/shard_map/all_gather | solution.py:41
  7.3 165.1 %all-gather.6.cloned.1.call-start = ((), (), s32[]{:S(2)}) async-start(), calls=%async_computation.3 | async-start | bytes 11010048 | tf_op jit(solution)/shard_map/all_gather | solution.py:42
  15.7 142.9 %all-to-all-start = ((bf16[64,10,2048]{2,1,0:T(8,128)(2,1)}), bf16[64,10,2048]{2,1,0:T(8,128)(2,1)}, u32[]{:S(2)}, u32[]{:S(2)}) async-start(bf16[64,10,2048]{2,1,0:T(8,128)(2,1)} %bitcast.16), calls=%async_computation | async-start | bytes 8388608 | tf_op jit(solution)/shard_map/all_to_all | solution.py:37
  33.9 148.5 %all-gather.8.cloned.1.call-start = ((), (), s32[]{:S(2)}) async-start(), calls=%async_computation.4 | async-start | bytes 11010048 | tf_op jit(solution)/shard_map/all_gather | solution.py:44
  182.4 5.4 %copy-start.5 = (bf16[640,1792]{1,0:T(8,128)(2,1)S(1)}, bf16[640,1792]{1,0:T(8,128)(2,1)}, u32[]{:S(2)}) copy-start(bf16[640,1792]{1,0:T(8,128)(2,1)} %multiply_convert_fusion) | copy-start | bytes 6881284
  182.4 5.4 %copy-start.4 = (bf16[1792,2048]{1,0:T(8,128)(2,1)S(1)}, bf16[1792,2048]{1,0:T(8,128)(2,1)}, u32[]{:S(2)}) copy-start(bf16[1792,2048]{1,0:T(8,128)(2,1)} %all-gather.8.cloned.1.call-done) | copy-start | bytes 22020100
  194.9 9.6 %copy-start.3 = (f32[64,2]{0,1:T(2,128)S(1)}, f32[64,2]{0,1:T(2,128)}, u32[]{:S(2)}) copy-start(f32[64,2]{0,1:T(2,128)} %param.10) | copy-start | bytes 1540
  194.9 151.4 %all-to-all-start.1 = ((bf16[64,10,2048]{2,1,0:T(8,128)(2,1)}), bf16[64,10,2048]{2,1,0:T(8,128)(2,1)}, u32[]{:S(2)}, u32[]{:S(2)}) async-start(bf16[64,10,2048]{2,1,0:T(8,128)(2,1)} %reshape.113), calls=%async_computation.1 | async-start | bytes 8388608 | tf_op jit(solution)/shard_map/all_to_all | solution.py:60
Sparse Core Ops, SparseCore 0:
  9.2 30.9 all-gather.3
  42.0 26.3 all-gather.5
  70.2 26.4 all-gather.7
where the time goes:
time: 361 us; the launch traced here: 360 us
  waiting for transfers between devices  268 us (74%)
  starting transfers between devices  28.1 us (8%)
  matrix products  28.1 us (8%)
  local copies, waits for them, and re-layouts  15.2 us (4%)
  between operations  13.3 us (4%)
  other arithmetic  7.77 us (2%)
    all_to_all x1, waiting for transfers between devices, per_device(): lax.all_to_all(partial_value, 'ep', split_axis=0, concat_axis=0, tiled=True)  142 us
    all_to_all x1, waiting for transfers between devices, per_device(): lax.all_to_all(copies, 'ep', split_axis=0, concat_axis=0, tiled=True)  124 us
    all_to_all x1, starting transfers between devices, per_device(): lax.all_to_all(copies, 'ep', split_axis=0, concat_axis=0, tiled=True)  18.2 us
    dot_general x1, matrix products, per_device(): up_part = jnp.dot(arrived, up_all, preferred_element_type=jnp.float32)  10 us
    dot_general x1, matrix products, per_device(): gate_part = jnp.dot(arrived, gate_all, preferred_element_type=jnp.float32)  9.65 us
    all_to_all x1, starting transfers between devices, per_device(): lax.all_to_all(partial_value, 'ep', split_axis=0, concat_axis=0, tiled=True)  9.54 us
    dot_general x2, matrix products, per_device(): jnp.dot(hidden[:, lower:lower + block_width], down_all[lower:lower + bloc...  8.49 us
  transfers between devices with their start and end apart: 5, of which 2 were waited for; matrix products, arithmetic and copies ran while one was open for 9% of the time, Pallas kernels for 0%

commit v1 on v0

--- a/solution.py
+++ b/solution.py
@@ -4,6 +4,7 @@
 from jax.sharding import PartitionSpec as P
 
 GROUP = 4
+LANES = 128
 
 
 def layer_norm(tokens, norm_gain):
@@ -31,9 +32,10 @@
     source = jnp.arange(local_rows * picks, dtype=jnp.int32) // picks
     packed = jnp.zeros((experts * capacity, width), jnp.bfloat16).at[target].set(normed[source])
     copies = jnp.broadcast_to(
-        packed.reshape(experts, 1, capacity, width), (experts, GROUP, capacity, width)
+        packed.reshape(experts, 1, capacity * width // LANES, LANES),
+        (experts, GROUP, capacity * width // LANES, LANES),
     )
-    copies = copies.reshape(ep_devices, capacity, width)
+    copies = copies.reshape(ep_devices, capacity * width // LANES, LANES)
     arrived = lax.all_to_all(copies, "ep", split_axis=0, concat_axis=0, tiled=True).reshape(
         ep_devices * capacity, width
     )
@@ -56,9 +58,13 @@
                 preferred_element_type=jnp.float32,
             )
         )
-    partial_value = summed.astype(jnp.bfloat16).reshape(ep_devices, capacity, width)
+    partial_value = summed.astype(jnp.bfloat16).reshape(
+        ep_devices, capacity * width // LANES, LANES
+    )
     returned = lax.all_to_all(partial_value, "ep", split_axis=0, concat_axis=0, tiled=True)
-    grouped = jnp.sum(returned.reshape(experts, GROUP, capacity, width).astype(jnp.float32), 1)
+    grouped = jnp.sum(
+        returned.reshape(experts, GROUP, capacity * width // LANES, LANES).astype(jnp.float32), 1
+    )
     grouped = grouped.reshape(experts * capacity, width)
     picked = grouped[target] * gate_weights.reshape(-1)[:, None]
     return jnp.sum(picked.reshape(local_rows, picks, width), 1).astype(jnp.bfloat16)

time: 361 us -> 236 us (0.65)
  the two profiles are of different devices: /device:TPU:668 before, /device:TPU:646 now
where the time goes in v1:
time: 236 us
  waiting for transfers between devices  136 us (58%)
  starting transfers between devices  36 us (15%)
  matrix products  29.5 us (12%)
  local copies, waits for them, and re-layouts  15.3 us (6%)
  between operations  13.3 us (6%)
  other arithmetic  5.79 us (2%)
    all_to_all x1, waiting for transfers between devices, per_device(): lax.all_to_all(copies, 'ep', split_axis=0, concat_axis=0, tiled=True)  67.3 us
    all_to_all x1, waiting for transfers between devices, per_device(): lax.all_to_all(partial_value, 'ep', split_axis=0, concat_axis=0, tiled=True)  66.8 us
    all_to_all x1, starting transfers between devices, per_device(): lax.all_to_all(copies, 'ep', split_axis=0, concat_axis=0, tiled=True)  20 us
    all_to_all x1, starting transfers between devices, per_device(): lax.all_to_all(partial_value, 'ep', split_axis=0, concat_axis=0, tiled=True)  15.7 us
    dot_general x1, matrix products, per_device(): gate_part = jnp.dot(arrived, gate_all, preferred_element_type=jnp.float32)  11 us
    dot_general x1, matrix products, per_device(): up_part = jnp.dot(arrived, up_all, preferred_element_type=jnp.float32)  9.98 us
    dot_general x2, matrix products, per_device(): jnp.dot(hidden[:, lower:lower + block_width], down_all[lower:lower + bloc...  8.51 us
  transfers between devices with their start and end apart: 5, of which 2 were waited for; matrix products, arithmetic and copies ran while one was open for 13% of the time, Pallas kernels for 0%

profile of v1, /device:TPU:646, one launch (start us, length us, event | category | flops | bytes accessed | tf_op | source)
XLA Modules:
  0.0 236.0 jit_solution(13095121990100703261)
XLA Ops:
  6.6 0.7 all-gather.4.cloned.1.call-update
  7.4 0.7 all-gather.6.cloned.1.call-update
  9.2 0.2 fusion.14
  9.7 3.2 %scatter_custom_fusion = bf16[160,2048]{1,0:T(8,128)(2,1)S(1)} fusion(s32[128]{0:T(128)S(1)} %fusion.22, bf16[64,2048]{1,0:T(8,128)(2,1)S(1)} %fusion.16, s32[1024]{0:T(1024)S(1)} %pad_clamp_fusion.1, bf16[]{:T(256)} %constant.32.clone.1), kind=kCustom, calls=%fused_computation.22 | custom fusion | bytes 655362 | tf_op jit(solution)/shard_map/scatter | solution.py:33
  12.9 0.3 broadcast_in_dim.7
  13.2 1.9 broadcast_in_dim.8
  15.1 20.0 %all-to-all-start = ((bf16[64,160,128]{2,1,0:T(8,128)(2,1)}), bf16[64,160,128]{2,1,0:T(8,128)(2,1)S(1)}, u32[]{:S(2)}, u32[]{:S(2)}) async-start(bf16[64,160,128]{2,1,0:T(8,128)(2,1)} %bitcast.16), calls=%async_computation | async-start | bytes 5242880 | tf_op jit(solution)/shard_map/all_to_all | solution.py:39
  35.1 0.2 all-gather.8.cloned.1.call-start
  35.4 0.5 all-gather.8.cloned.1.call-update
  35.9 67.3 %all-to-all-done = bf16[64,160,128]{2,1,0:T(8,128)(2,1)S(1)} async-done(((bf16[64,160,128]{2,1,0:T(8,128)(2,1)}), bf16[64,160,128]{2,1,0:T(8,128)(2,1)S(1)}, u32[]{:S(2)}, u32[]{:S(2)}) %all-to-all-start) | async-done | bytes 2621472 | tf_op jit(solution)/shard_map/all_to_all | solution.py:39
  103.2 3.1 %reshape.112 = bf16[640,2048]{1,0:T(8,128)(2,1)} reshape(bf16[64,160,128]{2,1,0:T(8,128)(2,1)S(1)} %all-to-all-done) | data formatting | bytes 5242880 | tf_op jit(solution)/shard_map/reshape | solution.py:39
  106.3 11.0 %fusion.23 = f32[640,1792]{1,0:T(8,128)} fusion(bf16[640,2048]{1,0:T(8,128)(2,1)} %reshape.112, bf16[2048,1792]{1,0:T(8,128)(2,1)} %all-gather.4.cloned.1.call-done), kind=kOutput, calls=%fused_computation.42 | convolution fusion | flops 4697620480 | bytes 14548992 | tf_op jit(solution)/shard_map/dot_general | solution.py:47
  117.3 10.0 %multiply_convert_fusion = bf16[640,1792]{1,0:T(8,128)(2,1)} fusion(f32[640,1792]{1,0:T(8,128)} %fusion.23, bf16[640,2048]{1,0:T(8,128)(2,1)S(1)} %copy-done, bf16[2048,1792]{1,0:T(8,128)(2,1)} %all-gather.6.cloned.1.call-done), kind=kOutput, calls=%fused_computation.5 | convolution fusion | flops 4704501760 | bytes 16842752 | tf_op jit(solution)/shard_map/dot_general | solution.py:48
  127.3 5.4 %fusion.4 = bf16[640,2048]{1,0:T(8,128)(2,1)S(1)} fusion(bf16[1792,2048]{1,0:T(8,128)(2,1)} %all-gather.8.cloned.1.call-done, bf16[640,1792]{1,0:T(8,128)(2,1)} %multiply_convert_fusion), kind=kOutput, calls=%fused_computation.10 | convolution fusion | flops 2350120960 | bytes 7438336 | tf_op jit(solution)/shard_map/dot_general | solution.py:55
  132.7 3.1 %fusion.7 = bf16[640,2048]{1,0:T(8,128)(2,1)S(1)} fusion(bf16[1792,2048]{1,0:T(8,128)(2,1)S(1)} %copy-done.5, bf16[640,1792]{1,0:T(8,128)(2,1)S(1)} %copy-done.6), kind=kOutput, calls=%fused_computation.11 | convolution fusion | flops 2350120960 | bytes 7438336 | tf_op jit(solution)/shard_map/dot_general | solution.py:55
  135.8 1.1 add_convert_fusion
  136.9 3.1 %reshape.113 = bf16[64,160,128]{2,1,0:T(8,128)(2,1)} reshape(bf16[640,2048]{1,0:T(8,128)(2,1)S(1)} %add_convert_fusion) | data formatting | bytes 5242880 | tf_op jit(solution)/shard_map/reshape | solution.py:61
  140.1 15.7 %all-to-all-start.1 = ((bf16[64,160,128]{2,1,0:T(8,128)(2,1)}), bf16[64,160,128]{2,1,0:T(8,128)(2,1)S(1)}, u32[]{:S(2)}, u32[]{:S(2)}) async-start(bf16[64,160,128]{2,1,0:T(8,128)(2,1)} %reshape.113), calls=%async_computation.1 | async-start | bytes 5242880 | tf_op jit(solution)/shard_map/all_to_all | solution.py:64
  155.9 66.8 %all-to-all-done.1 = bf16[64,160,128]{2,1,0:T(8,128)(2,1)S(1)} async-done(((bf16[64,160,128]{2,1,0:T(8,128)(2,1)}), bf16[64,160,128]{2,1,0:T(8,128)(2,1)S(1)}, u32[]{:S(2)}, u32[]{:S(2)}) %all-to-all-start.1) | async-done | bytes 2621472 | tf_op jit(solution)/shard_map/all_to_all | solution.py:64
  222.6 1.4 convert_reduce_fusion
  224.1 1.5 reshape.114
  225.6 1.0 gather_fusion
  226.6 0.6 gather.10
  227.2 2.2 multiply_reduce_fusion
  (36 shorter events, 1.4 us)
Async XLA Ops:
  6.5 1.6 copy-start.3
  6.5 2.5 %copy-start.1 = (bf16[64,2048]{1,0:T(8,128)(2,1)S(1)}, bf16[64,2048]{1,0:T(8,128)(2,1)}, u32[]{:S(2)}) copy-start(bf16[64,2048]{1,0:T(8,128)(2,1)} %param.7) | copy-start | bytes 786436
  6.6 2.9 %copy-start.2 = (f32[2048]{0:T(1024)S(1)}, f32[2048]{0:T(1024)}, u32[]{:S(2)}) copy-start(f32[2048]{0:T(1024)} %param.8) | copy-start | bytes 24580
  6.6 99.7 %all-gather.4.cloned.1.call-start = ((), (), s32[]{:S(2)}) async-start(), calls=%async_computation.2 | async-start | bytes 11010048 | tf_op jit(solution)/shard_map/all_gather | solution.py:43
  7.3 110.0 %all-gather.6.cloned.1.call-start = ((), (), s32[]{:S(2)}) async-start(), calls=%async_computation.3 | async-start | bytes 11010048 | tf_op jit(solution)/shard_map/all_gather | solution.py:44
  15.1 88.1 %all-to-all-start = ((bf16[64,160,128]{2,1,0:T(8,128)(2,1)}), bf16[64,160,128]{2,1,0:T(8,128)(2,1)S(1)}, u32[]{:S(2)}, u32[]{:S(2)}) async-start(bf16[64,160,128]{2,1,0:T(8,128)(2,1)} %bitcast.16), calls=%async_computation | async-start | bytes 5242880 | tf_op jit(solution)/shard_map/all_to_all | solution.py:39
  35.1 92.2 %all-gather.8.cloned.1.call-start = ((), (), s32[]{:S(2)}) async-start(), calls=%async_computation.4 | async-start | bytes 11010048 | tf_op jit(solution)/shard_map/all_gather | solution.py:46
  106.3 11.1 %copy-start = (bf16[640,2048]{1,0:T(8,128)(2,1)S(1)}, bf16[640,2048]{1,0:T(8,128)(2,1)}, u32[]{:S(2)}) copy-start(bf16[640,2048]{1,0:T(8,128)(2,1)} %reshape.112) | copy-start | bytes 7864324
  127.3 5.4 %copy-start.6 = (bf16[640,1792]{1,0:T(8,128)(2,1)S(1)}, bf16[640,1792]{1,0:T(8,128)(2,1)}, u32[]{:S(2)}) copy-start(bf16[640,1792]{1,0:T(8,128)(2,1)} %multiply_convert_fusion) | copy-start | bytes 6881284
  127.3 5.4 %copy-start.5 = (bf16[1792,2048]{1,0:T(8,128)(2,1)S(1)}, bf16[1792,2048]{1,0:T(8,128)(2,1)}, u32[]{:S(2)}) copy-start(bf16[1792,2048]{1,0:T(8,128)(2,1)} %all-gather.8.cloned.1.call-done) | copy-start | bytes 22020100
  140.1 15.7 %copy-start.4 = (f32[64,2]{0,1:T(2,128)S(1)}, f32[64,2]{0,1:T(2,128)}, u32[]{:S(2)}) copy-start(f32[64,2]{0,1:T(2,128)} %param.10) | copy-start | bytes 1540
  140.1 82.6 %all-to-all-start.1 = ((bf16[64,160,128]{2,1,0:T(8,128)(2,1)}), bf16[64,160,128]{2,1,0:T(8,128)(2,1)S(1)}, u32[]{:S(2)}, u32[]{:S(2)}) async-start(bf16[64,160,128]{2,1,0:T(8,128)(2,1)} %reshape.113), calls=%async_computation.1 | async-start | bytes 5242880 | tf_op jit(solution)/shard_map/all_to_all | solution.py:64
Sparse Core Ops, SparseCore 0:
  9.2 32.6 all-gather.3
  43.7 26.3 all-gather.5
  71.9 26.4 all-gather.7
